TPU v7x, 32 devices: a whole 2x2x4 slice. The times are simulated.
32 devices in a mesh: fs: 8 (over z, y), tp: 4 (over x, core).
Axes of the slice: x: 2, y: 2, z: 4, core: 2. Of those that a mesh axis runs over, the one named last changes fastest.
Arguments:
- prompt_tokens: bfloat16 [4, 128, 4096], P('tp'), may hold values from -6 to 6
- trained_up: float32 [4096, 16384], P('fs', 'tp'), may hold values from -0.09375 to 0.09375
- trained_down: float32 [16384, 4096], P('fs', 'tp'), may hold values from -0.046875 to 0.046875
- pre_gain: float32 [4096], P('fs'), may hold values from 0.1 to 1.9
- post_gain: float32 [4096], replicated, may hold values from 0.1 to 1.9
Outputs:
- layer_out: bfloat16 [4, 128, 4096], P('tp', 'fs')
- sampler_up: bfloat16 [4096, 16384], P(None, 'fs')
- sampler_down: bfloat16 [16384, 4096], P('fs')
All inputs are finite; a program needn't handle non-finite values.
Results may differ from a plain program's by a relative error of at most 0.0081.
Values may be sent and summed in bfloat16 or wider, within the bound.
A program may use at most 128 MiB of HBM per device.

v0:
```python
import jax
import jax.numpy as jnp
from jax import lax
from jax.sharding import PartitionSpec as P


def row_norm(values):
    return values * lax.rsqrt(jnp.mean(values * values, axis=-1, keepdims=True) + 1e-06)


def on_device(prompt_tokens, trained_up, trained_down, pre_gain, post_gain):
    folded = (pre_gain[:, None] * trained_up).astype(jnp.bfloat16)
    quarter = lax.all_to_all(folded, "tp", split_axis=0, concat_axis=1, tiled=True)
    owned = lax.all_to_all(quarter, "fs", split_axis=1, concat_axis=0, tiled=True)
    joined = lax.all_gather(owned, "tp", axis=0, tiled=True)
    n_fs = lax.axis_size("fs")
    n_tp = lax.axis_size("tp")
    width = joined.shape[1]
    joined = joined.reshape(n_tp, n_fs, joined.shape[0] // (n_tp * n_fs), width)
    sampler_up = jnp.transpose(joined, (1, 0, 2, 3)).reshape(-1, width)
    sampler_down = lax.all_gather(trained_down.astype(jnp.bfloat16), "tp", axis=1, tiled=True)
    flat = prompt_tokens[0].astype(jnp.float32)
    normed = row_norm(flat).astype(jnp.bfloat16)
    upward = jnp.dot(normed, sampler_up, preferred_element_type=jnp.float32)
    hidden = jnp.square(jax.nn.relu(upward)).astype(jnp.bfloat16)
    summed = lax.psum_scatter(
        jnp.dot(hidden, sampler_down, preferred_element_type=jnp.float32),
        "fs",
        scatter_dimension=0,
        tiled=True,
    )
    layer_out = (row_norm(summed) * post_gain).astype(jnp.bfloat16)
    return (layer_out[None], sampler_up, sampler_down)


def solution(mesh):
    placed = (P("tp", None, None), P("fs", "tp"), P("fs", "tp"), P("fs"), P())
    return jax.shard_map(
        on_device,
        mesh=mesh,
        in_specs=placed,
        out_specs=(P("tp", "fs", None), P(None, "fs"), P("fs", None)),
        check_vma=False,
    )
```

profile of v0, /device:TPU:0, one launch (start us, length us, event | category | flops | bytes accessed | tf_op | source)
XLA Modules:
  0.0 497.2 jit_solution(667741849209752609)
XLA Ops:
  7.2 0.0 all-gather.3.cloned.1.call-start
  7.2 4.6 multiply_convert_fusion
  11.8 52.3 %all_to_all.35 = bf16[4,128,4096]{2,1,0:T(8,128)(2,1)} all-to-all(bf16[4,128,4096]{2,1,0:T(8,128)(2,1)S(1)} %bitcast.25), channel_id=1, replica_groups=mesh['fs'=8,'tp'=4] {'tp'}, dimensions={0} | all-to-all | bytes 8388608 | tf_op jit(solution)/shard_map/all_to_all | solution.py:13
  64.1 6.3 %copy.9 = bf16[128,4,4096]{0,2,1:T(8,128)(2,1)} copy(bf16[128,4,4096]{2,0,1:T(8,128)(2,1)} %bitcast.22) | data formatting | bytes 8388608 | tf_op jit(solution)/shard_map/all_to_all | solution.py:13
  70.4 99.7 %all_to_all.36 = bf16[128,8,2048]{0,2,1:T(8,128)(2,1)} all-to-all(bf16[128,8,2048]{0,2,1:T(8,128)(2,1)} %bitcast.23), channel_id=1, replica_groups=mesh['fs'=8,'tp'=4] {'fs'}, dimensions={1} | all-to-all | bytes 8388608 | tf_op jit(solution)/shard_map/all_to_all | solution.py:14
  170.1 6.4 %copy.10 = bf16[8,128,2048]{2,1,0:T(8,128)(2,1)} copy(bf16[8,128,2048]{1,2,0:T(8,128)(2,1)} %bitcast.24) | data formatting | bytes 8388608 | tf_op jit(solution)/shard_map/all_to_all | solution.py:14
  176.6 0.0 all-gather.3.cloned.1.call-update
  176.6 0.0 copy-start
  176.6 0.0 all-gather.5.cloned.1.call-start
  176.7 6.3 %convert_element_type.28 = bf16[2048,1024]{1,0:T(8,128)(2,1)} convert(f32[2048,1024]{1,0:T(8,128)} %param.7) | non-fusion elementwise | flops 2097152 | bytes 12582912 | tf_op jit(solution)/shard_map/convert_element_type | solution.py:21
  182.9 0.0 all-gather.5.cloned.1.call-update
  182.9 0.0 reduce-scatter.2.cloned.1.call-start
  183.0 0.0 copy-done
  183.0 0.3 fusion.2
  183.3 97.5 %all-gather.3.cloned.1.call-done = bf16[4096,2048]{1,0:T(8,128)(2,1)} async-done(((bf16[1024,2048]{1,0:T(8,128)(2,1)}), bf16[4096,2048]{1,0:T(8,128)(2,1)}) %all-gather.3.cloned.1.call-update) | async-done | bytes 16777232 | tf_op jit(solution)/shard_map/all_gather | solution.py:15
  280.8 14.7 %copy.11 = bf16[8,4,128,2048]{3,2,1,0:T(8,128)(2,1)} copy(bf16[8,4,128,2048]{3,2,0,1:T(8,128)(2,1)} %bitcast.20) | data formatting | bytes 33554432 | tf_op jit(solution)/shard_map/transpose | solution.py:20
  295.5 93.3 %all-gather.5.cloned.1.call-done = bf16[2048,4096]{1,0:T(8,128)(2,1)} async-done(((bf16[2048,1024]{1,0:T(8,128)(2,1)}), bf16[2048,4096]{1,0:T(8,128)(2,1)}) %all-gather.5.cloned.1.call-update) | async-done | bytes 16777232 | tf_op jit(solution)/shard_map/all_gather | solution.py:21
  388.9 0.0 copy-start.1
  388.9 16.4 %fusion.8 = f32[128,4096]{1,0:T(8,128)} fusion(bf16[2048,4096]{1,0:T(8,128)(2,1)} %all-gather.5.cloned.1.call-done, bf16[4096,2048]{1,0:T(8,128)(2,1)} %bitcast.18, bf16[1,128,4096]{2,1,0:T(8,128)(2,1)S(1)} %copy-done, f32[128]{0:T(128)S(1)} %add_rsqrt_fusion.1), kind=kOutput, calls=%fused_computation.10 | convolution fusion | flops 4297326592 | bytes 36700672 | tf_op jit(solution)/shard_map/dot_general | solution.py:27
  405.3 0.0 reduce-scatter.2.cloned.1.call-update
  405.3 68.5 %reduce-scatter.2.cloned.1.call-done = f32[16,4096]{1,0:T(8,128)} async-done(((f32[128,4096]{1,0:T(8,128)}), f32[16,4096]{1,0:T(8,128)}) %reduce-scatter.2.cloned.1.call-update) | async-done | bytes 262160 | tf_op jit(solution)/shard_map/reduce_scatter | solution.py:26
  473.9 1.1 multiply_reduce_fusion
  475.0 0.0 copy-done.1
  475.0 1.7 fusion.11
  476.7 14.1 %copy.13 = bf16[2048,4096]{1,0:T(8,128)(2,1)} copy(bf16[2048,4096]{1,0:T(8,128)(2,1)} %all-gather.5.cloned.1.call-done) | data formatting | bytes 33554432
  (2 shorter events, 0.0 us)
Async XLA Ops:
  7.2 273.6 %all-gather.3.cloned.1.call-start = ((), (), s32[]{:S(2)}) async-start(), calls=%async_computation.3 | async-start | bytes 20971520 | tf_op jit(solution)/shard_map/all_gather | solution.py:15
  176.6 6.4 %copy-start = (bf16[1,128,4096]{2,1,0:T(8,128)(2,1)S(1)}, bf16[1,128,4096]{2,1,0:T(8,128)(2,1)}, u32[]{:S(2)}) copy-start(bf16[1,128,4096]{2,1,0:T(8,128)(2,1)} %param.5) | copy-start | bytes 3145732
  176.6 212.2 %all-gather.5.cloned.1.call-start = ((), (), s32[]{:S(2)}) async-start(), calls=%async_computation.4 | async-start | bytes 20971520 | tf_op jit(solution)/shard_map/all_gather | solution.py:21
  182.9 290.9 %reduce-scatter.2.cloned.1.call-start = ((), (), s32[]{:S(2)}) async-start(), calls=%async_computation.5 | async-start | bytes 2359296 | tf_op jit(solution)/shard_map/reduce_scatter | solution.py:26
  388.9 86.1 %copy-start.1 = (f32[4096]{0:T(1024)S(1)}, f32[4096]{0:T(1024)}, u32[]{:S(2)}) copy-start(f32[4096]{0:T(1024)} %param.9) | copy-start | bytes 49156
Sparse Core Ops, SparseCore 0:
  176.7 104.0 all-gather.2
  282.9 105.8 all-gather.4
  405.4 68.3 reduce-scatter.1
where the time goes:
time: 498 us; the launch traced here: 497 us
  waiting for transfers between devices  259 us (52%)
  blocking collectives  152 us (31%)
  local copies, waits for them, and re-layouts  41.5 us (8%)
  matrix products  16.4 us (3%)
  other arithmetic  14 us (3%)
  between operations  13.8 us (3%)
    all_to_all x1, blocking collectives, on_device(): lax.all_to_all(quarter, 'fs', split_axis=1, concat_axis=0, tiled=True)  99.7 us
    all_gather x1, waiting for transfers between devices, on_device(): joined = lax.all_gather(owned, 'tp', axis=0, tiled=True)  97.5 us
    all_gather x1, waiting for transfers between devices, on_device(): lax.all_gather(trained_down.astype(jnp.bfloat16), 'tp', axis=1, tiled=True)  93.3 us
    reduce_scatter x1, waiting for transfers between devices, on_device(): lax.psum_scatter(jnp.dot(hidden, sampler_down, preferred_element_type=jnp...  68.5 us
    all_to_all x1, blocking collectives, on_device(): lax.all_to_all(folded, 'tp', split_axis=0, concat_axis=1, tiled=True)  52.3 us
    dot_general x1, matrix products, on_device(): jnp.dot(hidden, sampler_down, preferred_element_type=jnp.float32)  16.4 us
    transpose x1, local copies, waits for them, and re-layouts, on_device(): sampler_up = jnp.transpose(joined, (1, 0, 2, 3)).reshape(-1, width)  14.7 us
    unnamed x5, local copies, waits for them, and re-layouts  14.1 us
  transfers between devices with their start and end apart: 3, of which 3 were waited for; matrix products, arithmetic and copies ran while one was open for 4% of the time, Pallas kernels for 0%

commit v1 on v0

--- a/solution.py
+++ b/solution.py
@@ -12,7 +12,9 @@
     folded = (pre_gain[:, None] * trained_up).astype(jnp.bfloat16)
     quarter = lax.all_to_all(folded, "tp", split_axis=0, concat_axis=1, tiled=True)
     owned = lax.all_to_all(quarter, "fs", split_axis=1, concat_axis=0, tiled=True)
-    joined = lax.all_gather(owned, "tp", axis=0, tiled=True)
+    joined = jnp.concatenate(
+        lax.all_to_all(jnp.stack([owned] * lax.axis_size("tp")), "tp", 0, 0), axis=0
+    )
     n_fs = lax.axis_size("fs")
     n_tp = lax.axis_size("tp")
     width = joined.shape[1]

time: 498 us -> 543 us (1.090)
  blocking collectives: 152 us -> 193 us
  waiting for transfers between devices: 259 us -> 249 us
  starting transfers between devices: 0.12 us -> 7.18 us
  local copies, waits for them, and re-layouts: 41.5 us -> 48.4 us
    all_to_all x0 -> x1, waiting for transfers between devices: none -> 183 us  [on_device(): lax.all_to_all(jnp.stack([owned] * lax.axis_size('tp')), 'tp', 0, 0)]
    all_gather x1 -> x0, waiting for transfers between devices: 97.5 us -> none  [on_device(): joined = lax.all_gather(owned, 'tp', axis=0, tiled=True)]
    all_gather x1, waiting for transfers between devices: 93.3 us -> 0.01 us  [on_device(): lax.all_gather(trained_down.astype(jnp.bfloat16), 'tp', axis=1, tiled=True)]
    all_to_all x1, blocking collectives: 52.3 us -> 93.1 us  [on_device(): lax.all_to_all(folded, 'tp', split_axis=0, concat_axis=1, tiled=True)]
    another operation x0 -> x1, local copies, waits for them, and re-layouts: none -> 7.44 us  [on_device(): jnp.stack([owned] * lax.axis_size('tp'))]
    all_to_all x0 -> x1, starting transfers between devices: none -> 7.1 us  [on_device(): lax.all_to_all(jnp.stack([owned] * lax.axis_size('tp')), 'tp', 0, 0)]
    unnamed x5 -> x7, local copies, waits for them, and re-layouts: 14.1 us -> 14.1 us
  transfers between devices with their start and end apart: 3 -> 3, of which waited for: 3 -> 2; matrix products, arithmetic and copies ran while one was open for 4% -> 7% of each run, Pallas kernels for 0% -> 0%
where the time goes in v1:
time: 543 us; the launch traced here: 542 us
  waiting for transfers between devices  249 us (46%)
  blocking collectives  193 us (36%)
  local copies, waits for them, and re-layouts  48.4 us (9%)
  matrix products  16.4 us (3%)
  between operations  14.1 us (3%)
  other arithmetic  13.8 us (3%)
  starting transfers between devices  7.18 us (1%)
    all_to_all x1, waiting for transfers between devices, on_device(): lax.all_to_all(jnp.stack([owned] * lax.axis_size('tp')), 'tp', 0, 0)  183 us
    all_to_all x1, blocking collectives, on_device(): lax.all_to_all(quarter, 'fs', split_axis=1, concat_axis=0, tiled=True)  100 us
    all_to_all x1, blocking collectives, on_device(): lax.all_to_all(folded, 'tp', split_axis=0, concat_axis=1, tiled=True)  93.1 us
    reduce_scatter x1, waiting for transfers between devices, on_device(): lax.psum_scatter(jnp.dot(hidden, sampler_down, preferred_element_type=jnp...  66.3 us
    dot_general x1, matrix products, on_device(): jnp.dot(hidden, sampler_down, preferred_element_type=jnp.float32)  16.4 us
    transpose x1, local copies, waits for them, and re-layouts, on_device(): sampler_up = jnp.transpose(joined, (1, 0, 2, 3)).reshape(-1, width)  14.2 us
    unnamed x7, local copies, waits for them, and re-layouts  14.1 us
  transfers between devices with their start and end apart: 3, of which 2 were waited for; matrix products, arithmetic and copies ran while one was open for 7% of the time, Pallas kernels for 0%

profile of v1, /device:TPU:0, one launch (start us, length us, event | category | flops | bytes accessed | tf_op | source)
XLA Modules:
  0.0 542.1 jit_solution(11014088258566491424)
XLA Ops:
  7.2 0.0 copy-start.2
  7.2 0.0 all-gather.2.cloned.1.call-start
  7.2 6.1 %convert_element_type.28 = bf16[2048,1024]{1,0:T(8,128)(2,1)} convert(f32[2048,1024]{1,0:T(8,128)} %param.7) | non-fusion elementwise | flops 2097152 | bytes 12582912 | tf_op jit(solution)/shard_map/convert_element_type | solution.py:23
  13.3 0.0 all-gather.2.cloned.1.call-update
  13.3 0.0 copy-done.2
  13.4 4.6 multiply_convert_fusion
  17.9 93.1 %all_to_all.37 = bf16[4,128,4096]{2,1,0:T(8,128)(2,1)} all-to-all(bf16[4,128,4096]{2,1,0:T(8,128)(2,1)S(1)} %bitcast.24), channel_id=1, replica_groups=mesh['fs'=8,'tp'=4] {'tp'}, dimensions={0} | all-to-all | bytes 8388608 | tf_op jit(solution)/shard_map/all_to_all | solution.py:13
  111.0 6.3 %copy.9 = bf16[128,4,4096]{0,2,1:T(8,128)(2,1)} copy(bf16[128,4,4096]{2,0,1:T(8,128)(2,1)} %bitcast.21) | data formatting | bytes 8388608 | tf_op jit(solution)/shard_map/all_to_all | solution.py:13
  117.4 100.1 %all_to_all.38 = bf16[128,8,2048]{0,2,1:T(8,128)(2,1)} all-to-all(bf16[128,8,2048]{0,2,1:T(8,128)(2,1)} %bitcast.22), channel_id=1, replica_groups=mesh['fs'=8,'tp'=4] {'fs'}, dimensions={1} | all-to-all | bytes 8388608 | tf_op jit(solution)/shard_map/all_to_all | solution.py:14
  217.5 6.4 %copy.10 = bf16[8,128,2048]{2,1,0:T(8,128)(2,1)} copy(bf16[8,128,2048]{1,2,0:T(8,128)(2,1)} %bitcast.23) | data formatting | bytes 8388608 | tf_op jit(solution)/shard_map/all_to_all | solution.py:14
  223.9 7.4 %stack.10 = bf16[4,1024,2048]{2,1,0:T(8,128)(2,1)} broadcast(bf16[1024,2048]{1,0:T(8,128)(2,1)} %bitcast.20), dimensions={1,2} | broadcast | bytes 20971520 | tf_op jit(solution)/shard_map/stack | solution.py:16
  231.3 0.0 copy-start
  231.3 7.1 %all-to-all-start.2 = ((bf16[4,1024,2048]{2,1,0:T(8,128)(2,1)}), bf16[4,1024,2048]{2,1,0:T(8,128)(2,1)}, u32[]{:S(2)}, u32[]{:S(2)}) async-start(bf16[4,1024,2048]{2,1,0:T(8,128)(2,1)} %stack.10), calls=%async_computation.2 | async-start | bytes 33554432 | tf_op jit(solution)/shard_map/all_to_all | solution.py:16
  238.5 0.0 reduce-scatter.2.cloned.1.call-start
  238.5 0.0 copy-done
  238.5 0.3 fusion.2
  238.8 182.7 %all-to-all-done.2 = bf16[4,1024,2048]{2,1,0:T(8,128)(2,1)} async-done(((bf16[4,1024,2048]{2,1,0:T(8,128)(2,1)}), bf16[4,1024,2048]{2,1,0:T(8,128)(2,1)}, u32[]{:S(2)}, u32[]{:S(2)}) %all-to-all-start.2) | async-done | bytes 16777248 | tf_op jit(solution)/shard_map/all_to_all | solution.py:16
  421.5 14.2 %copy.11 = bf16[8,4,128,2048]{3,2,1,0:T(8,128)(2,1)} copy(bf16[8,4,128,2048]{3,2,0,1:T(8,128)(2,1)} %bitcast.7) | data formatting | bytes 33554432 | tf_op jit(solution)/shard_map/transpose | solution.py:22
  435.6 0.0 all-gather.2.cloned.1.call-done
  435.6 0.0 copy-start.1
  435.6 16.4 %fusion.8 = f32[128,4096]{1,0:T(8,128)} fusion(bf16[2048,4096]{1,0:T(8,128)(2,1)} %all-gather.2.cloned.1.call-done, bf16[4096,2048]{1,0:T(8,128)(2,1)} %bitcast.18, bf16[1,128,4096]{2,1,0:T(8,128)(2,1)S(1)} %copy-done, f32[128]{0:T(128)S(1)} %add_rsqrt_fusion.1), kind=kOutput, calls=%fused_computation.10 | convolution fusion | flops 4297326592 | bytes 36700672 | tf_op jit(solution)/shard_map/dot_general | solution.py:29
  452.1 0.0 reduce-scatter.2.cloned.1.call-update
  452.1 66.3 %reduce-scatter.2.cloned.1.call-done = f32[16,4096]{1,0:T(8,128)} async-done(((f32[128,4096]{1,0:T(8,128)}), f32[16,4096]{1,0:T(8,128)}) %reduce-scatter.2.cloned.1.call-update) | async-done | bytes 262160 | tf_op jit(solution)/shard_map/reduce_scatter | solution.py:28
  518.4 1.1 multiply_reduce_fusion
  519.5 0.0 copy-done.1
  519.5 1.7 fusion.11
  521.2 14.1 %copy.13 = bf16[2048,4096]{1,0:T(8,128)(2,1)} copy(bf16[2048,4096]{1,0:T(8,128)(2,1)} %all-gather.2.cloned.1.call-done) | data formatting | bytes 33554432
  (2 shorter events, 0.0 us)
Async XLA Ops:
  7.2 6.2 %copy-start.2 = (f32[512]{0:T(512)S(1)}, f32[512]{0:T(512)}, u32[]{:S(2)}) copy-start(f32[512]{0:T(512)} %param.8) | copy-start | bytes 6148
  7.2 428.5 %all-gather.2.cloned.1.call-start = ((), (), s32[]{:S(2)}) async-start(), calls=%async_computation.4 | async-start | bytes 20971520 | tf_op jit(solution)/shard_map/all_gather | solution.py:23
  231.3 7.2 %copy-start = (bf16[1,128,4096]{2,1,0:T(8,128)(2,1)S(1)}, bf16[1,128,4096]{2,1,0:T(8,128)(2,1)}, u32[]{:S(2)}) copy-start(bf16[1,128,4096]{2,1,0:T(8,128)(2,1)} %param.5) | copy-start | bytes 3145732
  231.3 190.1 %all-to-all-start.2 = ((bf16[4,1024,2048]{2,1,0:T(8,128)(2,1)}), bf16[4,1024,2048]{2,1,0:T(8,128)(2,1)}, u32[]{:S(2)}, u32[]{:S(2)}) async-start(bf16[4,1024,2048]{2,1,0:T(8,128)(2,1)} %stack.10), calls=%async_computation.2 | async-start | bytes 33554432 | tf_op jit(solution)/shard_map/all_to_all | solution.py:16
  238.5 279.9 %reduce-scatter.2.cloned.1.call-start = ((), (), s32[]{:S(2)}) async-start(), calls=%async_computation.5 | async-start | bytes 2359296 | tf_op jit(solution)/shard_map/reduce_scatter | solution.py:28
  435.6 83.9 %copy-start.1 = (f32[4096]{0:T(1024)S(1)}, f32[4096]{0:T(1024)}, u32[]{:S(2)}) copy-start(f32[4096]{0:T(1024)} %param.9) | copy-start | bytes 49156
Sparse Core Ops, SparseCore 0:
  13.5 148.6 all-gather.1
  452.2 66.1 reduce-scatter.1

commit v2 on v0

--- a/solution.py
+++ b/solution.py
@@ -18,7 +18,7 @@
     width = joined.shape[1]
     joined = joined.reshape(n_tp, n_fs, joined.shape[0] // (n_tp * n_fs), width)
     sampler_up = jnp.transpose(joined, (1, 0, 2, 3)).reshape(-1, width)
-    sampler_down = lax.all_gather(trained_down.astype(jnp.bfloat16), "tp", axis=1, tiled=True)
+    sampler_down = jnp.concatenate(lax.all_gather(trained_down.astype(jnp.bfloat16), "tp"), axis=1)
     flat = prompt_tokens[0].astype(jnp.float32)
     normed = row_norm(flat).astype(jnp.bfloat16)
     upward = jnp.dot(normed, sampler_up, preferred_element_type=jnp.float32)

time: 498 us -> 437 us (0.88)
  waiting for transfers between devices: 259 us -> 143 us
  blocking collectives: 152 us -> 193 us
  local copies, waits for them, and re-layouts: 41.5 us -> 56.5 us
    all_gather x1, waiting for transfers between devices: 93.3 us -> 0.02 us  [on_device(): lax.all_gather(trained_down.astype(jnp.bfloat16), 'tp')]
    all_to_all x1, blocking collectives: 52.3 us -> 93.2 us  [on_device(): lax.all_to_all(folded, 'tp', split_axis=0, concat_axis=1, tiled=True)]
    all_gather x1, waiting for transfers between devices: 97.5 us -> 74.1 us  [on_device(): joined = lax.all_gather(owned, 'tp', axis=0, tiled=True)]
    all_gather x0 -> x1, local copies, waits for them, and re-layouts: none -> 19.1 us  [on_device(): lax.all_gather(trained_down.astype(jnp.bfloat16), 'tp')]
    unnamed x5 -> x7, local copies, waits for them, and re-layouts: 14.1 us -> 10.3 us
  transfers between devices with their start and end apart: 3 -> 3, of which waited for: 3 -> 2; matrix products, arithmetic and copies ran while one was open for 4% -> 11% of each run, Pallas kernels for 0% -> 0%
where the time goes in v2:
time: 437 us
  blocking collectives  193 us (44%)
  waiting for transfers between devices  143 us (33%)
  local copies, waits for them, and re-layouts  56.5 us (13%)
  matrix products  16.4 us (4%)
  between operations  13.8 us (3%)
  other arithmetic  13.7 us (3%)
    all_to_all x1, blocking collectives, on_device(): lax.all_to_all(quarter, 'fs', split_axis=1, concat_axis=0, tiled=True)  100 us
    all_to_all x1, blocking collectives, on_device(): lax.all_to_all(folded, 'tp', split_axis=0, concat_axis=1, tiled=True)  93.2 us
    all_gather x1, waiting for transfers between devices, on_device(): joined = lax.all_gather(owned, 'tp', axis=0, tiled=True)  74.1 us
    reduce_scatter x1, waiting for transfers between devices, on_device(): lax.psum_scatter(jnp.dot(hidden, sampler_down, preferred_element_type=jnp...  68.7 us
    all_gather x1, local copies, waits for them, and re-layouts, on_device(): lax.all_gather(trained_down.astype(jnp.bfloat16), 'tp')  19.1 us
    dot_general x1, matrix products, on_device(): jnp.dot(hidden, sampler_down, preferred_element_type=jnp.float32)  16.4 us
    transpose x1, local copies, waits for them, and re-layouts, on_device(): sampler_up = jnp.transpose(joined, (1, 0, 2, 3)).reshape(-1, width)  14.2 us
    unnamed x7, local copies, waits for them, and re-layouts  10.3 us
  transfers between devices with their start and end apart: 3, of which 2 were waited for; matrix products, arithmetic and copies ran while one was open for 11% of the time, Pallas kernels for 0%

profile of v2, /device:TPU:0, one launch (start us, length us, event | category | flops | bytes accessed | tf_op | source)
XLA Modules:
  0.0 436.8 jit_solution(10299181796042101305)
XLA Ops:
  7.2 0.0 copy-start.2
  7.2 0.0 all-gather.6.cloned.1.call-start
  7.2 6.1 %convert_element_type.28 = bf16[2048,1024]{1,0:T(8,128)(2,1)} convert(f32[2048,1024]{1,0:T(8,128)} %param.7) | non-fusion elementwise | flops 2097152 | bytes 12582912 | tf_op jit(solution)/shard_map/convert_element_type | solution.py:21
  13.3 0.0 all-gather.6.cloned.1.call-update
  13.3 0.0 all-gather.4.cloned.1.call-start
  13.4 0.0 copy-done.2
  13.4 4.6 %multiply_convert_fusion = bf16[512,4096]{1,0:T(8,128)(2,1)S(1)} fusion(f32[512,4096]{1,0:T(8,128)} %param.6, f32[512]{0:T(512)S(1)} %copy-done.2), kind=kLoop, calls=%fused_computation | loop fusion | flops 4194304 | bytes 12584960 | tf_op jit(solution)/shard_map/convert_element_type | solution.py:12
  18.0 93.2 %all_to_all.35 = bf16[4,128,4096]{2,1,0:T(8,128)(2,1)} all-to-all(bf16[4,128,4096]{2,1,0:T(8,128)(2,1)S(1)} %bitcast.33), channel_id=1, replica_groups=mesh['fs'=8,'tp'=4] {'tp'}, dimensions={0} | all-to-all | bytes 8388608 | tf_op jit(solution)/shard_map/all_to_all | solution.py:13
  111.1 6.3 %copy.11 = bf16[128,4,4096]{0,2,1:T(8,128)(2,1)} copy(bf16[128,4,4096]{2,0,1:T(8,128)(2,1)} %bitcast.30) | data formatting | bytes 8388608 | tf_op jit(solution)/shard_map/all_to_all | solution.py:13
  117.4 100.1 %all_to_all.36 = bf16[128,8,2048]{0,2,1:T(8,128)(2,1)} all-to-all(bf16[128,8,2048]{0,2,1:T(8,128)(2,1)} %bitcast.31), channel_id=1, replica_groups=mesh['fs'=8,'tp'=4] {'fs'}, dimensions={1} | all-to-all | bytes 8388608 | tf_op jit(solution)/shard_map/all_to_all | solution.py:14
  217.5 0.0 copy-start
  217.5 6.6 %copy.12 = bf16[8,128,2048]{2,1,0:T(8,128)(2,1)} copy(bf16[8,128,2048]{1,2,0:T(8,128)(2,1)} %bitcast.32) | data formatting | bytes 8388608 | tf_op jit(solution)/shard_map/all_to_all | solution.py:14
  224.2 0.0 all-gather.4.cloned.1.call-update
  224.2 0.0 reduce-scatter.2.cloned.1.call-start
  224.2 0.0 copy-done
  224.2 0.3 fusion.2
  224.5 0.0 all-gather.6.cloned.1.call-done
  224.6 19.1 %copy.14 = bf16[4,2048,1024]{2,0,1:T(4,128)(2,1)S(1)} copy(bf16[4,2048,1024]{2,1,0:T(8,128)(2,1)} %bitcast.27) | data formatting | bytes 33554432 | tf_op jit(solution)/shard_map/all_gather | solution.py:21
  243.7 10.3 %copy.15 = bf16[256,8,4,1024]{3,1,2,0:T(8,128)(2,1)} copy(bf16[256,8,4,1024]{3,2,1,0:T(4,128)(2,1)S(1)} %bitcast.26) | data formatting | bytes 33554432
  253.9 74.1 %all-gather.4.cloned.1.call-done = bf16[4096,2048]{1,0:T(8,128)(2,1)} async-done(((bf16[1024,2048]{1,0:T(8,128)(2,1)}), bf16[4096,2048]{1,0:T(8,128)(2,1)}) %all-gather.4.cloned.1.call-update) | async-done | bytes 16777232 | tf_op jit(solution)/shard_map/all_gather | solution.py:15
  328.1 14.2 %copy.13 = bf16[8,4,128,2048]{3,2,1,0:T(8,128)(2,1)} copy(bf16[8,4,128,2048]{3,2,0,1:T(8,128)(2,1)} %bitcast.28) | data formatting | bytes 33554432 | tf_op jit(solution)/shard_map/transpose | solution.py:20
  342.3 0.0 copy-start.1
  342.3 16.4 %fusion.8 = f32[128,4096]{1,0:T(8,128)} fusion(bf16[2048,4096]{1,0:T(8,128)(2,1)} %bitcast.22, bf16[4096,2048]{1,0:T(8,128)(2,1)} %bitcast.24, bf16[1,128,4096]{2,1,0:T(8,128)(2,1)S(1)} %copy-done, f32[128]{0:T(128)S(1)} %add_rsqrt_fusion.1), kind=kOutput, calls=%fused_computation.10 | convolution fusion | flops 4297326592 | bytes 36700672 | tf_op jit(solution)/shard_map/dot_general | solution.py:27
  358.7 0.0 reduce-scatter.2.cloned.1.call-update
  358.7 68.7 %reduce-scatter.2.cloned.1.call-done = f32[16,4096]{1,0:T(8,128)} async-done(((f32[128,4096]{1,0:T(8,128)}), f32[16,4096]{1,0:T(8,128)}) %reduce-scatter.2.cloned.1.call-update) | async-done | bytes 262160 | tf_op jit(solution)/shard_map/reduce_scatter | solution.py:26
  427.5 1.1 multiply_reduce_fusion
  428.6 0.0 copy-done.1
  428.6 1.7 fusion.11
  (2 shorter events, 0.0 us)
Async XLA Ops:
  7.2 6.2 %copy-start.2 = (f32[512]{0:T(512)S(1)}, f32[512]{0:T(512)}, u32[]{:S(2)}) copy-start(f32[512]{0:T(512)} %param.8) | copy-start | bytes 6148
  7.2 217.4 %all-gather.6.cloned.1.call-start = ((), (), s32[]{:S(2)}) async-start(), calls=%async_computation.5 | async-start | bytes 20971520 | tf_op jit(solution)/shard_map/all_gather | solution.py:21
  13.3 314.8 %all-gather.4.cloned.1.call-start = ((), (), s32[]{:S(2)}) async-start(), calls=%async_computation.3 | async-start | bytes 20971520 | tf_op jit(solution)/shard_map/all_gather | solution.py:15
  217.5 6.7 %copy-start = (bf16[1,128,4096]{2,1,0:T(8,128)(2,1)S(1)}, bf16[1,128,4096]{2,1,0:T(8,128)(2,1)}, u32[]{:S(2)}) copy-start(bf16[1,128,4096]{2,1,0:T(8,128)(2,1)} %param.5) | copy-start | bytes 3145732
  224.2 203.3 %reduce-scatter.2.cloned.1.call-start = ((), (), s32[]{:S(2)}) async-start(), calls=%async_computation.4 | async-start | bytes 2359296 | tf_op jit(solution)/shard_map/reduce_scatter | solution.py:26
  342.3 86.3 %copy-start.1 = (f32[4096]{0:T(1024)S(1)}, f32[4096]{0:T(1024)}, u32[]{:S(2)}) copy-start(f32[4096]{0:T(1024)} %param.9) | copy-start | bytes 49156
Sparse Core Ops, SparseCore 0:
  13.4 148.6 all-gather.5
  224.3 103.7 all-gather.3
  358.8 68.5 reduce-scatter.1
